TPU v7x, 32 devices: a whole 2x2x4 slice. The times are simulated.
32 devices in a mesh: fs: 4 (over z), rep: 4 (over y, x), tp: 2 (over core).
Axes of the slice: x: 2, y: 2, z: 4, core: 2. Of those that a mesh axis runs over, the one named last changes fastest.
Arguments:
- saved_input: bfloat16 [32768, 2048], P(('fs', 'rep')), may hold values from -8 to 8
- query_cotangent: bfloat16 [32768, 1024], P(('fs', 'rep'), 'tp'), may hold values from -0.03125 to 0.03125
- saved_heads: bfloat16 [32768, 1024], P(('fs', 'rep'), 'tp'), may hold values from -6 to 6
- block_cotangent: bfloat16 [32768, 2048], P(('fs', 'rep')), may hold values from -0.046875 to 0.046875
- query_weight: float32 [2048, 1024], P(('fs', 'rep'), 'tp'), may hold values from -6 to 6
- output_weight: float32 [1024, 2048], P('tp', ('fs', 'rep')), may hold values from -6 to 6
- query_factor: bfloat16 [2048, 256], P(('fs', 'rep')), may hold values from -0.125 to 0.125
- output_factor: bfloat16 [2048, 256], P(('fs', 'rep')), may hold values from -0.125 to 0.125
- query_first: float32 [256, 1024], P(None, 'tp'), may hold values from -6 to 6
- query_second: float32 [256, 1024], P(None, 'tp'), may hold values from 0.5 to 2
- output_first: float32 [1024, 256], P('tp'), may hold values from -6 to 6
- output_second: float32 [1024, 256], P('tp'), may hold values from 0.5 to 2
Outputs:
- new_query_weight: float32 [2048, 1024], P(('fs', 'rep'), 'tp')
- new_output_weight: float32 [1024, 2048], P('tp', ('fs', 'rep'))
- new_query_first: float32 [256, 1024], P(None, 'tp')
- new_query_second: float32 [256, 1024], P(None, 'tp')
- new_output_first: float32 [1024, 256], P('tp')
- new_output_second: float32 [1024, 256], P('tp')
- query_step: float32 [2048, 1024], P(('fs', 'rep'), 'tp')
- output_step: float32 [1024, 2048], P('tp', ('fs', 'rep'))
- query_copy: bfloat16 [2048, 1024], P(None, 'tp')
- output_copy: bfloat16 [1024, 2048], P('tp')
All inputs are finite; a program needn't handle non-finite values.
Results may differ from a plain program's by a relative error of at most 0.0013.
Values may be sent and summed in bfloat16 or wider, within the bound.
A program may use at most 128 MiB of HBM per device.

v0:
```python
import jax
import jax.numpy as jnp
from jax import lax
from jax.sharding import PartitionSpec as P

D = 2048
SBW = 1024


def split_parts(wide):
    upper = wide.astype(jnp.bfloat16)
    lower = (wide - upper.astype(jnp.float32)).astype(jnp.bfloat16)
    return (upper, lower)


def body(
    saved_input,
    query_cotangent,
    saved_heads,
    block_cotangent,
    query_weight,
    output_weight,
    query_factor,
    output_factor,
    query_first,
    query_second,
    output_first,
    output_second,
):
    contract = (((0,), (0,)), ((), ()))
    high = lax.Precision.HIGHEST
    factor_q = query_factor.astype(jnp.float32)
    factor_o = output_factor.astype(jnp.float32)
    whole_q, whole_o = (
        lax.all_gather(query_factor, ("fs", "rep"), axis=0, tiled=True),
        lax.all_gather(output_factor, ("fs", "rep"), axis=0, tiled=True),
    )
    input_low = jnp.dot(saved_input, whole_q, preferred_element_type=jnp.float32)
    cotan_low = jnp.dot(block_cotangent, whole_o, preferred_element_type=jnp.float32)
    input_upper, input_lower = split_parts(input_low)
    cotan_upper, cotan_lower = split_parts(cotan_low)
    part_query = lax.dot_general(
        input_upper, query_cotangent, contract, preferred_element_type=jnp.float32
    ) + lax.dot_general(input_lower, query_cotangent, contract, preferred_element_type=jnp.float32)
    part_output = lax.dot_general(
        saved_heads, cotan_upper, contract, preferred_element_type=jnp.float32
    ) + lax.dot_general(saved_heads, cotan_lower, contract, preferred_element_type=jnp.float32)
    query_proj, output_proj = lax.psum((part_query, part_output), ("fs", "rep"))
    new_query_first = 0.9 * query_first + 0.1 * query_proj
    new_output_first = 0.9 * output_first + 0.1 * output_proj
    new_query_second = 0.95 * query_second + 0.05 * query_proj * query_proj
    new_output_second = 0.95 * output_second + 0.05 * output_proj * output_proj
    query_dir = new_query_first / (jnp.sqrt(new_query_second) + 1e-08)
    output_dir = new_output_first / (jnp.sqrt(new_output_second) + 1e-08)
    query_raw = jnp.dot(factor_q, query_dir, precision=high)
    output_raw = jnp.dot(output_dir, factor_o.T, precision=high)
    query_sq, output_sq = lax.psum(
        (jnp.sum(query_raw * query_raw), jnp.sum(output_raw * output_raw)), ("fs", "rep", "tp")
    )
    entries = D * SBW
    query_step = query_raw / jnp.sqrt(query_sq / entries + 0.01)
    output_step = output_raw / jnp.sqrt(output_sq / entries + 0.01)
    new_query_weight = query_weight - 0.1 * query_step
    new_output_weight = output_weight - 0.1 * output_step
    query_copy, output_copy = (
        lax.all_gather(new_query_weight.astype(jnp.bfloat16), ("fs", "rep"), axis=0, tiled=True),
        lax.all_gather(new_output_weight.astype(jnp.bfloat16), ("fs", "rep"), axis=1, tiled=True),
    )
    return (
        new_query_weight,
        new_output_weight,
        new_query_first,
        new_query_second,
        new_output_first,
        new_output_second,
        query_step,
        output_step,
        query_copy,
        output_copy,
    )


def solution(mesh):
    in_specs = (
        P(("fs", "rep"), None),
        P(("fs", "rep"), "tp"),
        P(("fs", "rep"), "tp"),
        P(("fs", "rep"), None),
        P(("fs", "rep"), "tp"),
        P("tp", ("fs", "rep")),
        P(("fs", "rep"), None),
        P(("fs", "rep"), None),
        P(None, "tp"),
        P(None, "tp"),
        P("tp", None),
        P("tp", None),
    )
    out_specs = (
        P(("fs", "rep"), "tp"),
        P("tp", ("fs", "rep")),
        P(None, "tp"),
        P(None, "tp"),
        P("tp", None),
        P("tp", None),
        P(("fs", "rep"), "tp"),
        P("tp", ("fs", "rep")),
        P(None, "tp"),
        P("tp", None),
    )
    return jax.shard_map(body, mesh=mesh, in_specs=in_specs, out_specs=out_specs, check_vma=False)
```

profile of v0, /device:TPU:24, one launch (start us, length us, event | category | flops | bytes accessed | tf_op | source)
XLA Modules:
  0.0 426.7 jit_solution(4816327777482142928)
XLA Ops:
  7.2 0.0 copy-start
  7.2 0.0 all-gather.7.cloned.1.call-start
  7.2 0.7 all-gather.7.cloned.1.call-update
  7.9 0.0 all-gather.5.cloned.1.call-start
  8.0 0.7 all-gather.5.cloned.1.call-update
  8.7 0.0 all-reduce.4.cloned.1.call-start
  8.7 57.0 %all-gather.7.cloned.1.call-done = bf16[2048,256]{1,0:T(8,128)(2,1)} async-done(((bf16[128,256]{1,0:T(8,128)(2,1)}), bf16[2048,256]{1,0:T(8,128)(2,1)}) %all-gather.7.cloned.1.call-update) | async-done | bytes 1048592 | tf_op jit(solution)/shard_map/all_gather | solution.py:36
  65.7 6.1 %fusion.24 = f32[2048,256]{1,0:T(8,128)S(1)} fusion(bf16[2048,2048]{1,0:T(8,128)(2,1)} %param.15, bf16[2048,256]{1,0:T(8,128)(2,1)} %all-gather.7.cloned.1.call-done), kind=kOutput, calls=%fused_computation.38 | convolution fusion | flops 2147483648 | bytes 11534336 | tf_op jit(solution)/shard_map/dot_general | solution.py:39
  71.8 0.0 copy-done
  71.8 0.8 fusion.8
  72.6 1.6 fusion
  74.2 48.2 %all-gather.5.cloned.1.call-done = bf16[2048,256]{1,0:T(8,128)(2,1)} async-done(((bf16[128,256]{1,0:T(8,128)(2,1)}), bf16[2048,256]{1,0:T(8,128)(2,1)}) %all-gather.5.cloned.1.call-update) | async-done | bytes 1048592 | tf_op jit(solution)/shard_map/all_gather | solution.py:35
  122.4 0.0 copy-start.1
  122.4 6.2 %fusion.23 = f32[2048,256]{1,0:T(8,128)S(1)} fusion(bf16[2048,2048]{1,0:T(8,128)(2,1)} %param.12, bf16[2048,256]{1,0:T(8,128)(2,1)} %all-gather.5.cloned.1.call-done), kind=kOutput, calls=%fused_computation.37 | convolution fusion | flops 2147483648 | bytes 11534336 | tf_op jit(solution)/shard_map/dot_general | solution.py:38
  128.6 0.0 copy-done.1
  128.7 0.7 fusion.15
  129.4 0.0 copy-start.9
  129.4 0.0 copy-start.7
  129.4 1.5 convolution_add_fusion.1
  131.0 0.0 copy-start.8
  131.0 0.0 all-reduce.4.cloned.1.call-update
  131.0 0.0 all-gather.9.cloned.1.call-start
  131.0 0.0 copy-done.9
  131.1 0.8 copy.22
  131.9 0.0 copy-done.7
  131.9 1.0 copy.23
  132.9 0.0 copy-done.8
  132.9 0.0 copy-start.10
  132.9 1.0 copy.24
  133.9 108.6 %all-reduce.4.cloned.1.call-done = (f32[256,512]{1,0:T(8,128)}, f32[512,256]{0,1:T(8,128)}) async-done(((f32[256,512]{1,0:T(8,128)}, f32[512,256]{0,1:T(8,128)}), (f32[256,512]{1,0:T(8,128)}, f32[512,256]{0,1:T(8,128)})) %all-reduce.4.cloned.1.call-update) | async-done | bytes 1048592 | tf_op jit(solution)/shard_map/psum | solution.py:48
  242.4 0.0 copy-start.2
  242.4 0.0 copy-start.3
  242.4 0.0 copy-start.6
  242.4 1.7 fusion.2
  244.1 0.0 copy-done.10
  244.1 0.0 copy-start.11
  244.1 2.0 multiply_reduce_fusion
  246.1 0.0 copy-done.2
  246.1 0.0 copy-done.3
  246.1 0.0 copy-done.6
  246.2 0.2 fusion.1
  246.3 0.0 copy-start.4
  246.4 0.0 copy-start.5
  246.4 0.8 copy-done.4
  247.1 0.0 copy-done.11
  247.1 2.0 multiply_reduce_fusion.1
  249.2 0.0 copy-done.5
  249.2 39.4 %all-reduce = (f32[]{:T(128)}, f32[]{:T(128)}) all-reduce(f32[]{:T(128)} %get-tuple-element.34, f32[]{:T(128)} %get-tuple-element.36), channel_id=1, replica_groups=mesh['fs'=4,'rep'=4,'tp'=2] {'fs','rep','tp'}, use_global_device_ids=true, to_apply=%region_2.0 | all-reduce | flops 2 | bytes 16 | tf_op jit(solution)/shard_map/psum | solution.py:57
  289.3 1.8 fusion.22
  291.1 0.0 all-gather.9.cloned.1.call-update
  291.1 0.0 all-gather.11.cloned.1.call-start
  291.9 1.9 fusion.21
  293.8 0.0 all-gather.11.cloned.1.call-update
  293.8 1.0 copy.27
  294.8 1.0 copy.26
  295.8 1.8 copy.25
  297.6 0.8 copy.28
  298.4 54.9 %all-gather.9.cloned.1.call-done = bf16[2048,512]{0,1:T(8,128)(2,1)} async-done(((bf16[128,512]{0,1:T(8,128)(2,1)}), bf16[2048,512]{0,1:T(8,128)(2,1)}) %all-gather.9.cloned.1.call-update) | async-done | bytes 2097168 | tf_op jit(solution)/shard_map/all_gather | solution.py:66
  353.3 3.9 copy.29
  357.2 59.8 %all-gather.11.cloned.1.call-done = bf16[512,2048]{1,0:T(8,128)(2,1)} async-done(((bf16[512,128]{1,0:T(8,128)(2,1)}), bf16[512,2048]{1,0:T(8,128)(2,1)}) %all-gather.11.cloned.1.call-update) | async-done | bytes 2097168 | tf_op jit(solution)/shard_map/all_gather | solution.py:67
  417.0 3.2 copy.33
Async XLA Ops:
  7.2 64.6 %copy-start = (bf16[2048,512]{1,0:T(8,128)(2,1)S(1)}, bf16[2048,512]{1,0:T(8,128)(2,1)}, u32[]{:S(2)}) copy-start(bf16[2048,512]{1,0:T(8,128)(2,1)} %param.14) | copy-start | bytes 6291460
  7.2 58.5 %all-gather.7.cloned.1.call-start = ((), (), s32[]{:S(2)}) async-start(), calls=%async_computation.1 | async-start | bytes 1114112 | tf_op jit(solution)/shard_map/all_gather | solution.py:36
  7.9 114.5 %all-gather.5.cloned.1.call-start = ((), (), s32[]{:S(2)}) async-start(), calls=%async_computation | async-start | bytes 1114112 | tf_op jit(solution)/shard_map/all_gather | solution.py:35
  8.7 233.8 %all-reduce.4.cloned.1.call-start = ((), (), s32[]{:S(2)}) async-start(), calls=%async_computation.4 | async-start | bytes 2097152 | tf_op jit(solution)/shard_map/psum | solution.py:48
  122.4 6.2 %copy-start.1 = (bf16[2048,512]{1,0:T(8,128)(2,1)S(1)}, bf16[2048,512]{1,0:T(8,128)(2,1)}, u32[]{:S(2)}) copy-start(bf16[2048,512]{1,0:T(8,128)(2,1)} %param.13) | copy-start | bytes 6291460
  129.4 1.6 copy-start.9
  129.4 2.5 copy-start.7
  131.0 1.9 copy-start.8
  131.0 222.3 %all-gather.9.cloned.1.call-start = ((), (), s32[]{:S(2)}) async-start(), calls=%async_computation.2 | async-start | bytes 2228224 | tf_op jit(solution)/shard_map/all_gather | solution.py:66
  132.9 111.2 %copy-start.10 = (bf16[128,256]{1,0:T(8,128)(2,1)S(1)}, bf16[128,256]{1,0:T(8,128)(2,1)}, u32[]{:S(2)}) copy-start(bf16[128,256]{1,0:T(8,128)(2,1)} %param.19) | copy-start | bytes 196612
  242.4 3.7 copy-start.2
  242.4 3.7 copy-start.3
  242.4 3.7 copy-start.6
  244.1 3.0 copy-start.11
  246.3 0.8 copy-start.4
  246.4 2.8 copy-start.5
  291.1 125.9 %all-gather.11.cloned.1.call-start = ((), (), s32[]{:S(2)}) async-start(), calls=%async_computation.3 | async-start | bytes 2228224 | tf_op jit(solution)/shard_map/all_gather | solution.py:67
Sparse Core Ops, SparseCore 0:
  10.8 54.8 all-gather.6
  68.4 53.9 all-gather.4
  131.1 111.2 all-reduce.3
  291.2 62.0 all-gather.8
  355.9 61.1 all-gather.10
where the time goes:
time: 431 us; the launch traced here: 427 us
  waiting for transfers between devices  330 us (77%)
  blocking collectives  39.4 us (9%)
  matrix products  21 us (5%)
  local copies, waits for them, and re-layouts  15.3 us (4%)
  between operations  15.3 us (4%)
  other arithmetic  5.6 us (1%)
    psum x1, waiting for transfers between devices, body(): query_proj, output_proj = lax.psum((part_query, part_output), ('fs', 'rep'))  109 us
    all_gather x1, waiting for transfers between devices, body(): lax.all_gather(new_output_weight.astype(jnp.bfloat16), ('fs', 'rep'), axi...  59.8 us
    all_gather x1, waiting for transfers between devices, body(): lax.all_gather(output_factor, ('fs', 'rep'), axis=0, tiled=True)  57 us
    all_gather x1, waiting for transfers between devices, body(): lax.all_gather(new_query_weight.astype(jnp.bfloat16), ('fs', 'rep'), axis...  54.9 us
    all_gather x1, waiting for transfers between devices, body(): lax.all_gather(query_factor, ('fs', 'rep'), axis=0, tiled=True)  48.2 us
    psum x1, blocking collectives, body(): lax.psum((jnp.sum(query_raw * query_raw), jnp.sum(output_raw * output_raw...  39.4 us
    unnamed x33, local copies, waits for them, and re-layouts  15.3 us
  transfers between devices with their start and end apart: 5, of which 5 were waited for; matrix products, arithmetic and copies ran while one was open for 5% of the time, Pallas kernels for 0%

commit v1 on v0

v1 whole, which is shorter than its diff:
```python
import functools

import jax
import jax.numpy as jnp
from jax import lax
from jax.experimental import pallas as pl
from jax.experimental.pallas import tpu as pltpu
from jax.sharding import PartitionSpec as P

MESH = pl.DeviceIdType.MESH
BF = jnp.bfloat16
F32 = jnp.float32


def split_parts(wide):
    upper = wide.astype(BF)
    lower = (wide - upper.astype(F32)).astype(BF)
    return (upper, lower)


def remote(src, dst, send, recv, where):
    copy = pltpu.make_async_remote_copy(
        src_ref=src, dst_ref=dst, send_sem=send, recv_sem=recv, device_id=where, device_id_type=MESH
    )
    return copy


def place(nf, nr):
    f, r, t = lax.axis_index("fs"), lax.axis_index("rep"), lax.axis_index("tp")
    near = r + 1 - 2 * lax.rem(r, 2)
    side = lax.rem(r + 2, 4)
    far = 3 - r
    return f, r, t, near, side, far


def greet(nf, f, near, side, far, t):
    barrier = pltpu.get_barrier_semaphore()
    for df in range(1, nf):
        pl.semaphore_signal(barrier, inc=1, device_id={"fs": lax.rem(f + df, nf)}, device_id_type=MESH)
    for peer in (near, side, far):
        pl.semaphore_signal(barrier, inc=1, device_id={"rep": peer}, device_id_type=MESH)
    pl.semaphore_signal(barrier, inc=1, device_id={"tp": 1 - t}, device_id_type=MESH)
    pl.semaphore_wait(barrier, nf - 1 + 4)


def gather(nf, nr, f, r, near, side, far, parts, first, second, sems, passed=None):
    fs_s, fs_r, n_s, n_r, s_s, s_r, d_s, d_r = sems
    width = len(parts(0))
    half = len(first(0))
    me = f * nr + r
    sent = []

    def send(refs, send_sem, recv_sem, row, where):
        got = []
        for k, ref in enumerate(refs):
            copy = remote(ref, ref, send_sem.at[row, k], recv_sem.at[row, k], where)
            copy.start()
            got.append(copy)
        sent.extend(got)

    def arrive(refs, send_sem, recv_sem, row, where):
        for k, ref in enumerate(refs):
            remote(ref, ref, send_sem.at[row, k], recv_sem.at[row, k], where).wait_recv()

    send(parts(me), n_s, n_r, 0, {"rep": near})
    send(parts(me), s_s, s_r, 0, {"rep": side})
    for df in range(1, nf):
        send(parts(me), fs_s, fs_r, df, {"fs": lax.rem(f + df, nf)})
    for df in range(nf):
        from_f = lax.rem(f + nf - df, nf)
        if df > 0:
            slot = from_f * nr + r
            arrive(parts(slot), fs_s, fs_r, df, {"fs": from_f})
            send(parts(slot), n_s, n_r, df, {"rep": near})
            send(parts(slot), s_s, s_r, df, {"rep": side})
            if passed:
                passed(slot)
        if df > 0:
            relay(nf, nr, f, near, side, df - 1, parts, first, second, arrive, send, sems, passed)
    relay(nf, nr, f, near, side, nf - 1, parts, first, second, arrive, send, sems, passed)
    for df in range(nf):
        slot = lax.rem(f + nf - df, nf) * nr + far
        arrive(first(slot), d_s.at[0], d_r.at[0], df, {"rep": side})
        arrive(second(slot), d_s.at[1], d_r.at[1], df, {"rep": near})
        if passed:
            passed(slot)
    for copy in sent:
        copy.wait_send()


def relay(nf, nr, f, near, side, df, parts, first, second, arrive, send, sems, passed):
    fs_s, fs_r, n_s, n_r, s_s, s_r, d_s, d_r = sems
    from_f = lax.rem(f + nf - df, nf)
    one = from_f * nr + near
    arrive(parts(one), n_s, n_r, df, {"rep": near})
    send(first(one), d_s.at[0], d_r.at[0], df, {"rep": side})
    two = from_f * nr + side
    arrive(parts(two), s_s, s_r, df, {"rep": side})
    send(second(two), d_s.at[1], d_r.at[1], df, {"rep": near})
    if passed:
        passed(one)
        passed(two)


def gather_sems(nf, width, half):
    dma = pltpu.SemaphoreType.DMA
    return [dma((nf, width))] * 6 + [dma((2, nf, half))] * 2


def factor_kernel(nf, nr, fq_ref, fo_ref, out_ref, *sems):
    f, r, t, near, side, far = place(nf, nr)
    local, p_s, p_r = sems[8:]
    me = f * nr + r
    rows = fq_ref.shape[0]
    copies = [
        pltpu.make_async_copy(fq_ref, out_ref.at[0, me], local.at[0]),
        pltpu.make_async_copy(fo_ref, out_ref.at[1, me], local.at[1]),
    ]
    for copy in copies:
        copy.start()
    greet(nf, f, near, side, far, t)
    for copy in copies:
        copy.wait()
    relayed = []

    def passed(slot):
        copy = remote(
            out_ref.at[t, slot], out_ref.at[t, slot], p_s.at[len(relayed)], p_r.at[len(relayed)], {"tp": 1 - t}
        )
        copy.start()
        relayed.append(slot)

    gather(
        nf, nr, f, r, near, side, far,
        lambda s: [out_ref.at[t, s]],
        lambda s: [out_ref.at[t, s, pl.ds(0, rows // 2)]],
        lambda s: [out_ref.at[t, s, pl.ds(rows // 2, rows // 2)]],
        sems[:8],
        passed,
    )
    for k, slot in enumerate(relayed):
        copy = remote(out_ref.at[t, slot], out_ref.at[t, slot], p_s.at[k], p_r.at[k], {"tp": 1 - t})
        copy.wait_send()
        remote(out_ref.at[1 - t, slot], out_ref.at[1 - t, slot], p_s.at[k], p_r.at[k], {"tp": 1 - t}).wait_recv()


def update_kernel(
    nf, nr, wide,
    part_ref, factor_ref, wq_ref, wo_ref, fq_ref, sq_ref, fo_ref, so_ref,
    nwq_ref, nwo_ref, nfq_ref, nsq_ref, nfo_ref, nso_ref, stq_ref, sto_ref, cq_ref, co_ref,
    outgoing, landed, partial, exchanged, whole, dirs, square, *sems,
):
    f, r, t, near, side, far = place(nf, nr)
    a_s, a_r, b_s, b_r, c_s, c_r, e_s, e_r, x_s, x_r = sems[8:]
    n = nf * nr
    me = f * nr + r
    depth = factor_ref.shape[2]
    rank = dirs.shape[2]
    for k in range(nr):
        outgoing[k] = part_ref[k].astype(BF)
    greet(nf, f, near, side, far, t)
    sent = []
    peers = (near, side, far)
    for k, peer in enumerate(peers):
        copy = remote(outgoing.at[peer], landed.at[k], a_s.at[k], a_r.at[k], {"rep": peer})
        copy.start()
        sent.append(copy)
    for k, peer in enumerate(peers):
        remote(outgoing.at[peer], landed.at[k], a_s.at[k], a_r.at[k], {"rep": peer}).wait_recv()
    total = part_ref[r] + landed[0].astype(F32) + landed[1].astype(F32) + landed[2].astype(F32)
    partial[...] = total.astype(BF)
    for df in range(1, nf):
        to = lax.rem(f + df, nf)
        copy = remote(partial.at[to], exchanged.at[df], b_s.at[df], b_r.at[df], {"fs": to})
        copy.start()
        sent.append(copy)
    mine = part_ref[r, f] + landed[0, f].astype(F32) + landed[1, f].astype(F32) + landed[2, f].astype(F32)
    for df in range(1, nf):
        remote(partial.at[f], exchanged.at[df], b_s.at[df], b_r.at[df], {"fs": f}).wait_recv()
        mine = mine + exchanged[df].astype(F32)
    whole[r, f] = mine.astype(BF)
    for df in range(nf):
        from_f = lax.rem(f + nf - df, nf)
        if df == 0:
            for step in range(1, nf):
                copy = remote(
                    whole.at[r, f], whole.at[r, f], c_s.at[step], c_r.at[step], {"fs": lax.rem(f + step, nf)}
                )
                copy.start()
                sent.append(copy)
        else:
            ref = whole.at[r, from_f]
            remote(ref, ref, c_s.at[df], c_r.at[df], {"fs": from_f}).wait_recv()
        for k, peer in enumerate(peers):
            ref = whole.at[r, from_f]
            copy = remote(ref, ref, e_s.at[k, df], e_r.at[k, df], {"rep": peer})
            copy.start()
            sent.append(copy)
    for df in range(nf):
        from_f = lax.rem(f + nf - df, nf)
        for k, peer in enumerate(peers):
            ref = whole.at[peer, from_f]
            remote(ref, ref, e_s.at[k, df], e_r.at[k, df], {"rep": peer}).wait_recv()
    rows = nr // 2
    cols = part_ref.shape[3]
    for which, first, second, new_first, new_second in (
        (0, fq_ref, sq_ref, nfq_ref, nsq_ref),
        (1, fo_ref, so_ref, nfo_ref, nso_ref),
    ):
        proj = whole[which * rows : (which + 1) * rows].astype(F32).reshape(rank, cols)
        if which:
            proj = proj.T
        moved = 0.9 * first[...] + 0.1 * proj
        spread = 0.95 * second[...] + 0.05 * proj * proj
        new_first[...] = moved
        new_second[...] = spread
        way = moved / (jnp.sqrt(spread) + 1e-08)
        if which:
            way = way.T
        upper, lower = split_parts(way)
        dirs[which, 0] = upper
        dirs[which, 1] = lower

    def raw_of(which, slot):
        block = factor_ref[which, slot]
        return jnp.dot(block, dirs[which, 0], preferred_element_type=F32) + jnp.dot(
            block, dirs[which, 1], preferred_element_type=F32
        )

    for which in range(2):
        def add(slot, carry):
            raw = raw_of(which, slot)
            return carry + jnp.sum((raw * raw).reshape(depth // 8, 8, cols), axis=0)

        tally = lax.fori_loop(0, n, add, jnp.zeros((8, cols), F32))
        square[0, which] = tally
    copy = remote(square.at[0], square.at[1], x_s, x_r, {"tp": 1 - t})
    copy.start()
    raw_q = raw_of(0, me)
    raw_o = raw_of(1, me).T
    copy.wait()
    entries = wide * cols * 2
    sums = [
        jnp.sum(square[0, which] + square[1, which]) / entries + 0.01 for which in range(2)
    ]
    for raw, mean, weight, new_weight, step_ref, which in (
        (raw_q, sums[0], wq_ref, nwq_ref, stq_ref, 0),
        (raw_o, sums[1], wo_ref, nwo_ref, sto_ref, 1),
    ):
        step = raw / jnp.sqrt(jnp.full(raw.shape, mean, F32))
        new = weight[...] - 0.1 * step
        step_ref[...] = step
        new_weight[...] = new
        if which == 0:
            cq_ref[me] = new.astype(BF)
        elif depth % 128 == 0:
            co_ref[:, pl.ds(pl.multiple_of(me * depth, 128), depth)] = new.astype(BF)
        else:
            co_ref[me] = new.astype(BF)

    def output_slot(slot):
        if depth % 128 == 0:
            return co_ref.at[:, pl.ds(pl.multiple_of(slot * depth, 128), depth)]
        return co_ref.at[slot]

    gather(
        nf, nr, f, r, near, side, far,
        lambda s: [cq_ref.at[s], output_slot(s)],
        lambda s: [cq_ref.at[s]],
        lambda s: [output_slot(s)],
        sems[:8],
    )
    for copy in sent:
        copy.wait_send()


def body(
    nf, nr,
    saved_input, query_cotangent, saved_heads, block_cotangent, query_weight, output_weight,
    query_factor, output_factor, query_first, query_second, output_first, output_second,
):
    contract = (((0,), (0,)), ((), ()))
    n = nf * nr
    depth, rank = query_factor.shape
    cols = query_weight.shape[1]
    dma = pltpu.SemaphoreType.DMA
    vmem = pl.BlockSpec(memory_space=pltpu.VMEM)
    factors = pl.pallas_call(
        functools.partial(factor_kernel, nf, nr),
        out_shape=jax.ShapeDtypeStruct((2, n, depth, rank), BF),
        in_specs=[vmem] * 2,
        out_specs=vmem,
        scratch_shapes=gather_sems(nf, 1, 1) + [dma((2,)), dma((n,)), dma((n,))],
        compiler_params=pltpu.CompilerParams(collective_id=0, has_side_effects=True),
    )(query_factor, output_factor)
    whole_q = factors[0].reshape(n * depth, rank)
    whole_o = factors[1].reshape(n * depth, rank)
    input_low = jnp.dot(saved_input, whole_q, preferred_element_type=F32)
    cotan_low = jnp.dot(block_cotangent, whole_o, preferred_element_type=F32)
    input_upper, input_lower = split_parts(input_low)
    cotan_upper, cotan_lower = split_parts(cotan_low)
    part_query = lax.dot_general(
        input_upper, query_cotangent, contract, preferred_element_type=F32
    ) + lax.dot_general(input_lower, query_cotangent, contract, preferred_element_type=F32)
    part_output = lax.dot_general(
        cotan_upper, saved_heads, contract, preferred_element_type=F32
    ) + lax.dot_general(cotan_lower, saved_heads, contract, preferred_element_type=F32)
    rows = 2 * rank // n
    part = jnp.concatenate([part_query, part_output], axis=0).reshape(nr, nf, rows, cols)
    aligned = depth % 128 == 0
    shape = jax.ShapeDtypeStruct
    outs = pl.pallas_call(
        functools.partial(update_kernel, nf, nr, n * depth),
        out_shape=[
            shape((depth, cols), F32), shape((cols, depth), F32),
            shape((rank, cols), F32), shape((rank, cols), F32),
            shape((cols, rank), F32), shape((cols, rank), F32),
            shape((depth, cols), F32), shape((cols, depth), F32),
            shape((n, depth, cols), BF),
            shape((cols, n * depth) if aligned else (n, cols, depth), BF),
        ],
        in_specs=[vmem] * 8,
        out_specs=[vmem] * 10,
        scratch_shapes=[
            pltpu.VMEM((nr, nf, rows, cols), BF),
            pltpu.VMEM((3, nf, rows, cols), BF),
            pltpu.VMEM((nf, rows, cols), BF),
            pltpu.VMEM((nf, rows, cols), BF),
            pltpu.VMEM((nr, nf, rows, cols), BF),
            pltpu.VMEM((2, 2, rank, cols), BF),
            pltpu.VMEM((2, 2, 8, cols), F32),
        ]
        + gather_sems(nf, 2, 1)
        + [dma((3,)), dma((3,)), dma((nf,)), dma((nf,)), dma((nf,)), dma((nf,)), dma((3, nf)), dma((3, nf)), dma, dma],
        compiler_params=pltpu.CompilerParams(
            collective_id=1, has_side_effects=True, vmem_limit_bytes=60 * 1024 * 1024
        ),
    )(part, factors, query_weight, output_weight, query_first, query_second, output_first, output_second)
    *rest, query_copy, output_copy = outs
    query_copy = query_copy.reshape(n * depth, cols)
    if not aligned:
        output_copy = output_copy.transpose(1, 0, 2).reshape(cols, n * depth)
    return (*rest, query_copy, output_copy)


def solution(mesh):
    nf, nr = mesh.shape["fs"], mesh.shape["rep"]
    in_specs = (
        P(("fs", "rep"), None), P(("fs", "rep"), "tp"), P(("fs", "rep"), "tp"), P(("fs", "rep"), None),
        P(("fs", "rep"), "tp"), P("tp", ("fs", "rep")), P(("fs", "rep"), None), P(("fs", "rep"), None),
        P(None, "tp"), P(None, "tp"), P("tp", None), P("tp", None),
    )
    out_specs = (
        P(("fs", "rep"), "tp"), P("tp", ("fs", "rep")), P(None, "tp"), P(None, "tp"), P("tp", None), P("tp", None),
        P(("fs", "rep"), "tp"), P("tp", ("fs", "rep")), P(None, "tp"), P("tp", None),
    )
    return jax.shard_map(
        functools.partial(body, nf, nr), mesh=mesh, in_specs=in_specs, out_specs=out_specs, check_vma=False
    )
```

time: 431 us -> 135 us (0.31); the launches traced: 427 us -> 135 us
  waiting for transfers between devices: 330 us -> 0 us
  Pallas kernels: 0 us -> 107 us
  blocking collectives: 39.4 us -> 0 us
  between operations: 15.3 us -> 0.82 us
  matrix products: 21 us -> 11.1 us
  other arithmetic: 5.6 us -> 1.04 us
    all_gather x4 -> x0, waiting for transfers between devices: 220 us -> none  [the longest x1 59.8 us: body(): lax.all_gather(new_output_weight.astype(jnp.bfloat16), ('fs', 'rep'), axi...]
    psum x1 -> x0, waiting for transfers between devices: 109 us -> none  [body(): query_proj, output_proj = lax.psum((part_query, part_output), ('fs', 'rep'))]
    pallas_call x0 -> x2, Pallas kernels: none -> 107 us  [the longest x1 86.3 us: body(): pl.pallas_call(functools.partial(update_kernel, nf, nr, n * depth), out_s...]
    psum x1 -> x0, blocking collectives: 39.4 us -> none  [body(): lax.psum((jnp.sum(query_raw * query_raw), jnp.sum(output_raw * output_raw...]
    dot_general x6 -> x4, matrix products: 18.7 us -> 9.71 us  [the longest x1 5.92 us: body(): cotan_low = jnp.dot(block_cotangent, whole_o, preferred_element_type=F32)]
    unnamed x33 -> x32, local copies, waits for them, and re-layouts: 15.3 us -> 12.9 us
  transfers between devices with their start and end apart: 5 -> 0, of which waited for: 5 -> 0; matrix products, arithmetic and copies ran while one was open for 5% -> 0% of each run, Pallas kernels for 0% -> 0%
where the time goes in v1:
time: 135 us
  Pallas kernels  107 us (79%)
  local copies, waits for them, and re-layouts  14.8 us (11%)
  matrix products  11.1 us (8%)
    pallas_call x1, Pallas kernels, body(): pl.pallas_call(functools.partial(update_kernel, nf, nr, n * depth), out_s...  86.3 us
    pallas_call x1, Pallas kernels, body(): pl.pallas_call(functools.partial(factor_kernel, nf, nr), out_shape=jax.Sh...  21.2 us
    unnamed x32, local copies, waits for them, and re-layouts  12.9 us
    dot_general x1, matrix products, body(): cotan_low = jnp.dot(block_cotangent, whole_o, preferred_element_type=F32)  5.92 us

profile of v1, /device:TPU:24, one launch (start us, length us, event | category | flops | bytes accessed | tf_op | source)
XLA Modules:
  0.0 135.2 jit_solution(1711013608533653654)
XLA Ops:
  0.6 0.0 copy-start
  0.7 21.2 %shard_map.195.factor_ref = bf16[2,16,128,256]{3,2,1,0:T(8,128)(2,1)} custom-call(bf16[128,256]{1,0:T(8,128)(2,1)} %fq_ref.2, bf16[128,256]{1,0:T(8,128)(2,1)} %fo_ref.2), custom_call_target="tpu_custom_call" | custom-call | tf_op jit(solution)/shard_map/pallas_call | solution.py:288
  21.9 0.0 slice-start
  21.9 1.9 %fusion.6 = (bf16[1,16,128,256]{3,2,1,0:T(8,128)(2,1)S(1)}, bf16[1,16,128,256]{3,2,1,0:T(8,128)(2,1)S(1)}) fusion(bf16[2,16,128,256]{3,2,1,0:T(8,128)(2,1)} %shard_map.195.factor_ref), kind=kLoop, calls=%fused_computation.13 | loop fusion | bytes 4194304 | tf_op jit(solution)/shard_map/slice | solution.py:296
  23.8 0.0 slice-start.1
  23.8 5.9 %convolution_bitcast_fusion = f32[2048,256]{0,1:T(8,128)S(1)} fusion(bf16[2048,256]{1,0:T(8,128)(2,1)S(1)} %bitcast.19, bf16[2048,2048]{1,0:T(8,128)(2,1)} %param.15), kind=kOutput, calls=%fused_computation | convolution fusion | flops 2147483648 | bytes 11534336 | tf_op jit(solution)/shard_map/dot_general | solution.py:299
  29.7 0.0 copy-done
  29.7 0.7 fusion.1
  30.5 0.7 convolution_add_fusion
  31.2 0.0 slice-done
  31.2 0.0 slice-done.1
  31.2 0.0 copy-start.1
  31.2 2.4 %convolution_bitcast_fusion.1 = f32[2048,256]{0,1:T(8,128)S(1)} fusion(bf16[2048,256]{1,0:T(8,128)(2,1)S(1)} %bitcast.18, bf16[2048,2048]{1,0:T(8,128)(2,1)S(1)} %bitcast.21), kind=kOutput, calls=%fused_computation.1 | convolution fusion | flops 2147483648 | bytes 11534336 | tf_op jit(solution)/shard_map/dot_general | solution.py:298
  33.6 0.0 copy-done.1
  33.6 0.7 fusion.4
  34.3 0.7 convolution_add_fusion.1
  35.0 1.0 pad_maximum_fusion
  36.1 86.3 %shard_map.196 = (f32[128,512]{1,0:T(8,128)}, f32[512,128]{1,0:T(8,128)}, f32[256,512]{1,0:T(8,128)}, f32[256,512]{1,0:T(8,128)}, f32[512,256]{1,0:T(8,128)}, /*...) custom-call(f32[4,4,32,512]{3,2,1,0:T(8,128)} %bitcast.16, ...), custom_call_target="tpu_custom_call" | custom-call | tf_op jit(solution)/shard_map/pallas_call | solution.py:312
  122.3 0.0 copy-start.6
  122.4 0.0 copy-start.5
  122.4 0.0 copy-start.4
  122.4 1.8 %copy.32 = f32[128,512]{1,0:T(8,128)} copy(f32[128,512]{1,0:T(8,128)} %get-tuple-element.42) | data formatting | bytes 524288
  124.2 1.7 %copy.33 = f32[512,128]{1,0:T(8,128)} copy(f32[512,128]{1,0:T(8,128)} %get-tuple-element.43) | data formatting | bytes 524288
  125.8 0.0 copy-start.8
  125.8 1.9 %copy.34 = f32[256,512]{1,0:T(8,128)} copy(f32[256,512]{1,0:T(8,128)} %get-tuple-element.44) | data formatting | bytes 1048576
  127.7 0.0 copy-done.6
  127.7 0.0 copy-start.7
  127.8 0.0 copy-start.3
  127.8 0.8 copy.35
  128.5 0.0 copy-done.5
  128.5 0.8 copy.36
  129.3 0.0 copy-done.4
  129.3 0.8 copy.37
  130.1 0.0 copy-done.8
  130.1 0.7 copy.38
  130.8 0.0 copy-done.7
  130.8 0.7 copy.39
  131.6 0.0 copy-done.3
  131.6 0.0 copy-start.2
  131.6 1.3 copy.40
  132.9 1.0 copy-done.2
  133.9 1.3 copy.41
  (1 shorter events, 0.0 us)
Async XLA Ops:
  0.6 29.1 %copy-start = (bf16[2048,512]{1,0:T(8,128)(2,1)S(1)}, bf16[2048,512]{1,0:T(8,128)(2,1)}, u32[]{:S(2)}) copy-start(bf16[2048,512]{1,0:T(8,128)(2,1)} %param.14) | copy-start | bytes 6291460
  21.9 9.3 %slice-start = ((s8[8388608]{0:T(1024)(128)(4,1)}), s8[4194304]{0:T(1024)(128)(4,1)S(1)}, s32[]{:S(2)}) async-start(s8[8388608]{0:T(1024)(128)(4,1)} %bitcast.20), calls=%async_computation | async-start | bytes 8388608
  23.8 7.4 %slice-start.1 = ((s8[8388608]{0:T(1024)(128)(4,1)}), s8[4194304]{0:T(1024)(128)(4,1)S(1)}, s32[]{:S(2)}) async-start(s8[8388608]{0:T(1024)(128)(4,1)} %bitcast.20), calls=%async_computation.1 | async-start | bytes 8388608
  31.2 2.4 %copy-start.1 = (bf16[2048,512]{1,0:T(8,128)(2,1)S(1)}, bf16[2048,512]{1,0:T(8,128)(2,1)}, u32[]{:S(2)}) copy-start(bf16[2048,512]{1,0:T(8,128)(2,1)} %param.13) | copy-start | bytes 6291460
  122.3 5.4 %copy-start.6 = (f32[256,512]{1,0:T(8,128)S(1)}, f32[256,512]{1,0:T(8,128)}, u32[]{:S(2)}) copy-start(f32[256,512]{1,0:T(8,128)} %get-tuple-element.45) | copy-start | bytes 1572868
  122.4 6.2 %copy-start.5 = (f32[512,256]{1,0:T(8,128)S(1)}, f32[512,256]{1,0:T(8,128)}, u32[]{:S(2)}) copy-start(f32[512,256]{1,0:T(8,128)} %get-tuple-element.46) | copy-start | bytes 1572868
  122.4 7.0 %copy-start.4 = (f32[512,256]{1,0:T(8,128)S(1)}, f32[512,256]{1,0:T(8,128)}, u32[]{:S(2)}) copy-start(f32[512,256]{1,0:T(8,128)} %get-tuple-element.47) | copy-start | bytes 1572868
  125.8 4.3 %copy-start.8 = (f32[128,512]{1,0:T(8,128)S(1)}, f32[128,512]{1,0:T(8,128)}, u32[]{:S(2)}) copy-start(f32[128,512]{1,0:T(8,128)} %get-tuple-element.48) | copy-start | bytes 786436
  127.7 3.1 %copy-start.7 = (f32[512,128]{1,0:T(8,128)S(1)}, f32[512,128]{1,0:T(8,128)}, u32[]{:S(2)}) copy-start(f32[512,128]{1,0:T(8,128)} %get-tuple-element.49) | copy-start | bytes 786436
  127.8 3.8 %copy-start.3 = (bf16[16,128,512]{2,1,0:T(8,128)(2,1)S(1)}, bf16[16,128,512]{2,1,0:T(8,128)(2,1)}, u32[]{:S(2)}) copy-start(bf16[16,128,512]{2,1,0:T(8,128)(2,1)} %get-tuple-element.28) | copy-start | bytes 6291460
  131.6 2.3 %copy-start.2 = (bf16[512,2048]{1,0:T(8,128)(2,1)S(1)}, bf16[512,2048]{1,0:T(8,128)(2,1)}, u32[]{:S(2)}) copy-start(bf16[512,2048]{1,0:T(8,128)(2,1)} %get-tuple-element.51) | copy-start | bytes 6291460
